TPU v7x, 32 devices: a whole 2x2x4 slice. The times are simulated.
32 devices in a mesh: sp: 8 (over z, y), tp: 4 (over x, core).
Axes of the slice: x: 2, y: 2, z: 4, core: 2. Of those that a mesh axis runs over, the one named last changes fastest.
Arguments:
- queries: bfloat16 [8192, 1024], P('sp', 'tp'), may hold values from -300 to 300
- keys: bfloat16 [8192, 512], P('sp', 'tp'), may hold values from -6 to 6
- values: bfloat16 [8192, 512], P('sp', 'tp'), may hold values from -6 to 6
- sink_logits: float32 [16], P('tp'), may hold values from 1 to 6
- residual: bfloat16 [8192, 2048], P('sp'), may hold values from -3 to 3
- out_weight: bfloat16 [1024, 2048], P('tp'), may hold values from -0.5390625 to 0.5390625
- norm_gain: float32 [2048], replicated, may hold values from 0.1 to 1.9
- gate_weight: bfloat16 [2048, 5632], P('sp', 'tp'), may hold values from -0.125 to 0.125
- up_weight: bfloat16 [2048, 5632], P('sp', 'tp'), may hold values from -0.125 to 0.125
- down_weight: bfloat16 [2048, 5632], P('sp', 'tp'), may hold values from -0.1796875 to 0.1796875
Outputs:
- layer_out: bfloat16 [8192, 2048], P(('sp', 'tp'))
All inputs are finite; a program needn't handle non-finite values.
Results may differ from a plain program's by a relative error of at most 0.02.
Values may be sent and summed in bfloat16 or wider, within the bound.
A program may use at most 64 MiB of HBM per device.

v0:
```python
import jax
import jax.numpy as jnp
from jax import lax
from jax.sharding import PartitionSpec as P

QH = 16
HD = 64
WINDOW = 128


def shifted(block, axis, distance):
    devices = range(lax.axis_size(axis))
    route = [(i - distance, i) for i in devices if i - distance in devices]
    return lax.ppermute(block, axis, route)


def attend(queries, keys, values, sink_logits):
    local_rows = queries.shape[0]
    kv_local = keys.shape[1] // HD
    heads_local = queries.shape[1] // HD
    groups = heads_local // kv_local
    blocks = local_rows // WINDOW
    key_value = jnp.concatenate([keys, values], axis=1)
    previous = shifted(key_value[local_rows - WINDOW :], "sp", 1)
    extended = jnp.concatenate([previous, key_value], axis=0)
    stacked = extended.reshape(blocks + 1, WINDOW, 2 * kv_local * HD)
    band = jnp.concatenate([stacked[:-1], stacked[1:]], axis=1)
    key_band = band[:, :, : kv_local * HD].reshape(blocks, 2 * WINDOW, kv_local, HD)
    value_band = band[:, :, kv_local * HD :].reshape(blocks, 2 * WINDOW, kv_local, HD)
    query_blocks = queries.reshape(blocks, WINDOW, kv_local, groups, HD)
    query_index = jnp.arange(WINDOW, dtype=jnp.int32)[:, None]
    key_index = jnp.arange(2 * WINDOW, dtype=jnp.int32)[None, :]
    distance = query_index - key_index + WINDOW
    offset = lax.axis_index("sp") * local_rows
    key_place = (
        offset
        + jnp.arange(blocks, dtype=jnp.int32)[:, None, None] * WINDOW
        + key_index[None]
        - WINDOW
    )
    valid = (distance >= 0) & (distance < WINDOW) & (key_place >= 0)
    head_number = (
        lax.axis_index("tp") * heads_local + jnp.arange(heads_local, dtype=jnp.int32) + 1
    ).astype(jnp.float32)
    slopes = (2.0 ** (-8.0 * head_number / QH)).reshape(kv_local, groups, 1, 1, 1)
    scores = jnp.einsum(
        "nqhgd,nkhd->hgnqk", query_blocks, key_band, preferred_element_type=jnp.float32
    ) * HD ** (-0.5)
    scores = scores - slopes * distance.astype(jnp.float32)
    scores = jnp.where(valid, scores, -jnp.inf)
    sinks = sink_logits.reshape(kv_local, groups, 1, 1, 1)
    top = jnp.maximum(jnp.max(scores, axis=-1, keepdims=True), sinks)
    expd = jnp.exp(scores - top)
    denom = jnp.sum(expd, axis=-1, keepdims=True) + jnp.exp(sinks - top)
    weights = (expd / denom).astype(jnp.bfloat16)
    output = jnp.einsum(
        "hgnqk,nkhd->nqhgd", weights, value_band, preferred_element_type=jnp.float32
    )
    return output.reshape(local_rows, heads_local * HD).astype(jnp.bfloat16)


def rms_scale(rows, norm_gain):
    rows_f = rows.astype(jnp.float32)
    scale = lax.rsqrt(jnp.mean(rows_f * rows_f, axis=-1, keepdims=True) + 1e-06)
    return (rows_f * scale * norm_gain).astype(jnp.bfloat16)


def expand_rows(normed, gate_full, up_full):
    gate = jnp.dot(normed, gate_full, preferred_element_type=jnp.float32)
    upper = jnp.dot(normed, up_full, preferred_element_type=jnp.float32)
    return (jax.nn.silu(gate) * upper).astype(jnp.bfloat16)


def per_device(
    queries,
    keys,
    values,
    sink_logits,
    residual,
    out_weight,
    norm_gain,
    gate_weight,
    up_weight,
    down_weight,
):
    attended = attend(queries, keys, values, sink_logits)
    local_rows = queries.shape[0]
    tp_count = lax.axis_size("tp")
    own_rows = local_rows // tp_count
    first_row = lax.axis_index("tp") * own_rows
    partial_sum = jnp.dot(attended, out_weight, preferred_element_type=jnp.float32)
    projected = lax.psum(partial_sum.astype(jnp.bfloat16), "tp").astype(jnp.float32)
    mixed_all = (residual.astype(jnp.float32) + projected).astype(jnp.bfloat16)
    mixed_rows = lax.dynamic_slice_in_dim(mixed_all, first_row, own_rows, 0)
    gate_full, up_full = (
        lax.all_gather(gate_weight, "sp", axis=0, tiled=True),
        lax.all_gather(up_weight, "sp", axis=0, tiled=True),
    )
    hidden = expand_rows(rms_scale(mixed_all, norm_gain), gate_full, up_full)
    down_full = lax.all_gather(down_weight, "sp", axis=0, tiled=True)
    expanded = lax.psum_scatter(
        lax.dot_general(
            hidden, down_full, (((1,), (1,)), ((), ())), preferred_element_type=jnp.float32
        ).astype(jnp.bfloat16),
        "tp",
        scatter_dimension=0,
        tiled=True,
    ).astype(jnp.float32)
    return (mixed_rows.astype(jnp.float32) + 0.5 * expanded).astype(jnp.bfloat16)


def solution(mesh):
    return jax.shard_map(
        per_device,
        mesh=mesh,
        in_specs=(
            P("sp", "tp"),
            P("sp", "tp"),
            P("sp", "tp"),
            P("tp"),
            P("sp", None),
            P("tp", None),
            P(),
            P("sp", "tp"),
            P("sp", "tp"),
            P("sp", "tp"),
        ),
        out_specs=P(("sp", "tp"), None),
        check_vma=False,
    )
```

profile of v0, /device:TPU:1, one launch (start us, length us, event | category | flops | bytes accessed | tf_op | source)
XLA Modules:
  0.0 385.6 jit_solution(11114447815396450490)
XLA Ops:
  7.4 0.0 copy-start
  7.4 0.0 all-reduce.2.cloned.1.call-start
  7.4 1.1 constant_dynamic-update-slice_fusion.1
  8.5 1.0 constant_dynamic-update-slice_fusion
  9.5 4.0 %collective-permute-start = (bf16[128,256]{1,0:T(8,128)(2,1)S(1)}, bf16[128,256]{1,0:T(8,128)(2,1)S(1)}, u32[]{:S(2)}, u32[]{:S(2)}) collective-permute-start(bf16[128,256]{1,0:T(8,128)(2,1)S(1)} %slice.25), channel_id=1, source_target_pairs={{0,4},{4,8},{8,12},{12,16},{16,20},{20,24},{24,28},{1,5},{5,9},{9,... | collective-permute-start | bytes 196616 | tf_op jit(solution)/shard_map/ppermute | solution.py:14
  13.6 0.1 add_compare_fusion
  13.7 0.1 broadcast_multiply_fusion
  13.8 0.3 broadcast_and_fusion
  14.1 3.2 reshape.128
  17.3 0.7 max.18
  18.1 0.0 collective-permute-done
  18.1 0.3 pad_maximum_fusion
  18.4 0.2 copy.21
  18.6 2.3 fusion.5
  21.0 0.0 copy-start.1
  21.0 0.1 broadcast_maximum_fusion
  21.0 1.9 copy-done.1
  22.9 1.1 fusion.4
  24.0 0.1 exponential_add_fusion
  24.1 0.2 copy.20
  24.3 3.5 fusion.11
  27.8 0.3 copy.26
  28.1 0.0 copy-done
  28.1 3.3 convolution_convert_fusion.1
  31.5 0.0 all-reduce.2.cloned.1.call-update
  31.5 0.0 all-gather.4.cloned.1.call-start
  31.5 0.5 all-gather.4.cloned.1.call-update
  32.1 0.0 all-gather.6.cloned.1.call-start
  32.1 0.5 all-gather.6.cloned.1.call-update
  32.7 0.0 all-gather.8.cloned.1.call-start
  32.7 0.5 all-gather.8.cloned.1.call-update
  33.2 0.0 copy-start.2
  33.2 0.2 reduce-scatter.2.cloned.1.call-start
  33.5 83.9 %all-reduce.2.cloned.1.call-done = bf16[1024,2048]{1,0:T(8,128)(2,1)} async-done(((bf16[1024,2048]{1,0:T(8,128)(2,1)}), bf16[1024,2048]{1,0:T(8,128)(2,1)}) %all-reduce.2.cloned.1.call-update) | async-done | bytes 4194320 | tf_op jit(solution)/shard_map/psum | solution.py:92
  117.4 7.5 %fusion = (f32[1024]{0:T(1024)S(1)}, bf16[1024,2048]{1,0:T(8,128)(2,1)}) fusion(bf16[1024,2048]{1,0:T(8,128)(2,1)} %all-reduce.2.cloned.1.call-done, bf16[1024,2048]{1,0:T(8,128)(2,1)} %param.14), kind=kLoop, calls=%fused_computation.2 | loop fusion | flops 14679040 | bytes 12587008 | tf_op jit(solution)/shard_map/reduce_sum | solution.py:64
  124.8 0.4 all-gather.4.cloned.1.call-done
  125.2 0.0 copy-done.2
  125.2 11.9 %fusion.15 = f32[1024,1408]{1,0:T(8,128)} fusion(bf16[2048,1408]{1,0:T(8,128)(2,1)} %all-gather.4.cloned.1.call-done, bf16[1024,2048]{1,0:T(8,128)(2,1)} %get-tuple-element.6, f32[2048]{0:T(1024)S(1)} %copy-done.2, f32[1024]{0:T(1024)S(1)} %add_rsqrt_fusion), kind=kOutput, calls=%fused_computation.20 | convolution fusion | flops 5913968640 | bytes 15740928 | tf_op jit(solution)/shard_map/dot_general | solution.py:69
  137.1 80.4 %all-gather.6.cloned.1.call-done = bf16[2048,1408]{1,0:T(8,128)(2,1)} async-done(((bf16[256,1408]{1,0:T(8,128)(2,1)}), bf16[2048,1408]{1,0:T(8,128)(2,1)}) %all-gather.6.cloned.1.call-update) | async-done | bytes 5767184 | tf_op jit(solution)/shard_map/all_gather | solution.py:97
  217.6 92.4 %all-gather.8.cloned.1.call-done = bf16[2048,1408]{1,0:T(8,128)(2,1)} async-done(((bf16[256,1408]{1,0:T(8,128)(2,1)}), bf16[2048,1408]{1,0:T(8,128)(2,1)}) %all-gather.8.cloned.1.call-update) | async-done | bytes 5767184 | tf_op jit(solution)/shard_map/all_gather | solution.py:100
  309.9 20.8 %convolution_convert_fusion = bf16[1024,2048]{1,0:T(8,128)(2,1)} fusion(bf16[2048,1408]{1,0:T(8,128)(2,1)} %all-gather.8.cloned.1.call-done, f32[1024,1408]{1,0:T(8,128)} %fusion.15, bf16[2048,1408]{1,0:T(8,128)(2,1)} %all-gather.6.cloned.1.call-done, bf16[1024,2048]{1,0:T(8,128)(2,1)} %get-tuple-element.6, f32[2048]{0:T(1024)S(1)} %copy-done.2, ...), kind=kOutput, calls=%fused_computation.11 | convolution fusion | flops 11830296576 | bytes 25702400 | tf_op jit(solution)/shard_map/dot_general | solution.py:102
  330.7 0.0 reduce-scatter.2.cloned.1.call-update
  330.8 44.4 %reduce-scatter.2.cloned.1.call-done = bf16[256,2048]{1,0:T(8,128)(2,1)} async-done(((bf16[1024,2048]{1,0:T(8,128)(2,1)}), bf16[256,2048]{1,0:T(8,128)(2,1)}) %reduce-scatter.2.cloned.1.call-update) | async-done | bytes 1048592 | tf_op jit(solution)/shard_map/reduce_scatter | solution.py:101
  375.1 2.9 add_convert_fusion.1
  (7 shorter events, 0.1 us)
Async XLA Ops:
  7.4 20.8 %copy-start = (bf16[256,2048]{1,0:T(8,128)(2,1)S(1)}, bf16[256,2048]{1,0:T(8,128)(2,1)}, u32[]{:S(2)}) copy-start(bf16[256,2048]{1,0:T(8,128)(2,1)} %param.15) | copy-start | bytes 3145732
  7.4 110.0 %all-reduce.2.cloned.1.call-start = ((), (), s32[]{:S(2)}) async-start(), calls=%async_computation.1 | async-start | bytes 8388608 | tf_op jit(solution)/shard_map/psum | solution.py:92
  9.5 8.6 %collective-permute-start = (bf16[128,256]{1,0:T(8,128)(2,1)S(1)}, bf16[128,256]{1,0:T(8,128)(2,1)S(1)}, u32[]{:S(2)}, u32[]{:S(2)}) collective-permute-start(bf16[128,256]{1,0:T(8,128)(2,1)S(1)} %slice.25), channel_id=1, source_target_pairs={{0,4},{4,8},{8,12},{12,16},{16,20},{20,24},{24,28},{1,5},{5,9},{9,... | collective-permute-start | bytes 196616 | tf_op jit(solution)/shard_map/ppermute | solution.py:14
  21.0 1.9 copy-start.1
  31.5 93.7 %all-gather.4.cloned.1.call-start = ((), (), s32[]{:S(2)}) async-start(), calls=%async_computation.2 | async-start | bytes 6488064 | tf_op jit(solution)/shard_map/all_gather | solution.py:96
  32.1 185.5 %all-gather.6.cloned.1.call-start = ((), (), s32[]{:S(2)}) async-start(), calls=%async_computation.3 | async-start | bytes 6488064 | tf_op jit(solution)/shard_map/all_gather | solution.py:97
  32.7 277.3 %all-gather.8.cloned.1.call-start = ((), (), s32[]{:S(2)}) async-start(), calls=%async_computation.4 | async-start | bytes 6488064 | tf_op jit(solution)/shard_map/all_gather | solution.py:100
  33.2 92.0 %copy-start.2 = (f32[2048]{0:T(1024)S(1)}, f32[2048]{0:T(1024)}, u32[]{:S(2)}) copy-start(f32[2048]{0:T(1024)} %param.16) | copy-start | bytes 24580
  33.2 341.9 %reduce-scatter.2.cloned.1.call-start = ((), (), s32[]{:S(2)}) async-start(), calls=%async_computation.5 | async-start | bytes 5242880 | tf_op jit(solution)/shard_map/reduce_scatter | solution.py:101
Sparse Core Ops, SparseCore 0:
  31.6 85.7 all-reduce.1
  330.9 44.2 reduce-scatter.1
Sparse Core Ops, SparseCore 1:
  34.2 91.0 all-gather.3
  127.3 90.2 all-gather.5
  219.6 90.2 all-gather.7
where the time goes:
time: 387 us; the launch traced here: 386 us
  waiting for transfers between devices  303 us (78%)
  matrix products  41.9 us (11%)
  between operations  15.2 us (4%)
  other arithmetic  12.5 us (3%)
  local copies, waits for them, and re-layouts  8.71 us (2%)
  starting transfers between devices  4.31 us (1%)
    all_gather x1, waiting for transfers between devices, per_device(): down_full = lax.all_gather(down_weight, 'sp', axis=0, tiled=True)  92.4 us
    psum x1, waiting for transfers between devices, per_device(): lax.psum(partial_sum.astype(jnp.bfloat16), 'tp').astype(jnp.float32)  83.9 us
    all_gather x1, waiting for transfers between devices, per_device(): lax.all_gather(up_weight, 'sp', axis=0, tiled=True)  80.4 us
    reduce_scatter x1, waiting for transfers between devices, per_device(): lax.psum_scatter(lax.dot_general(hidden, down_full, (((1,), (1,)), ((), (...  44.4 us
    dot_general x1, matrix products, per_device(): lax.dot_general(hidden, down_full, (((1,), (1,)), ((), ())), preferred_el...  20.8 us
    dot_general x1, matrix products, expand_rows(): gate = jnp.dot(normed, gate_full, preferred_element_type=jnp.float32)  11.9 us
  transfers between devices with their start and end apart: 6, of which 5 were waited for; matrix products, arithmetic and copies ran while one was open for 6% of the time, Pallas kernels for 0%

commit v1 on v0

v1 whole, which is shorter than its diff:
```python
import functools

import jax
import jax.numpy as jnp
from jax import lax
from jax.experimental import pallas as pl
from jax.experimental.pallas import tpu as pltpu
from jax.sharding import PartitionSpec as P

QH = 16
HD = 64
WINDOW = 128
LAG = 2
GATE, UP, DOWN = 0, 1, 2
MESH = pl.DeviceIdType.MESH


def layer_kernel(
    zs,
    ys,
    tp,
    q_ref,
    k_ref,
    v_ref,
    sink_ref,
    res_hbm,
    ow_ref,
    gain_ref,
    gate_hbm,
    up_hbm,
    down_hbm,
    out_ref,
    weights,
    kext,
    vext,
    att,
    psend,
    precv,
    res,
    mixed,
    normed,
    hidden,
    esend,
    erecv,
    local_sem,
    halo_send,
    halo_recv,
    wsend,
    wrecv,
    rs_send,
    rs_recv,
    ag_send,
    ag_recv,
    ex_send,
    ex_recv,
):
    sp = zs * ys
    last = 2 * zs - 2
    me_sp = lax.axis_index("sp")
    me = lax.axis_index("tp")
    z = me_sp // ys
    y = me_sp % ys
    rows = q_ref.shape[0]
    own = rows // tp
    chunk = gate_hbm.shape[0]
    heads = q_ref.shape[1] // HD
    kvs = k_ref.shape[1] // HD
    groups = heads // kvs
    blocks = rows // WINDOW

    def block_rows(index, size):
        return pl.ds(pl.multiple_of(index * size, size), size)

    own_rows = block_rows(me, own)

    def piece(w, s, target, direction):
        part = weights.at[w, block_rows(s, chunk), :]
        return pltpu.make_async_remote_copy(
            src_ref=part,
            dst_ref=part,
            send_sem=wsend.at[w, s, direction],
            recv_sem=wrecv.at[w, s],
            device_id={"sp": target},
            device_id_type=MESH,
        )

    def offset(k):
        return ((k + 1) // 2) * (1 - 2 * (k % 2))

    def send_all(w, s, moves, drain):
        for condition, target, direction in moves:

            @pl.when(condition)
            def _():
                copy = piece(w, s, target, direction)
                if drain:
                    copy.wait_send()
                else:
                    copy.start()

    def zpart(k, ws, drain=False):
        off = offset(k)
        sz = z + off

        @pl.when((sz >= 0) & (sz < zs))
        def _():
            s = sz * ys + y
            for w in ws:
                if not drain:

                    @pl.when(k > 0)
                    def _():
                        piece(w, s, me_sp, 0).wait_recv()

                send_all(
                    w,
                    s,
                    (
                        ((off <= 0) & (z + 1 < zs), me_sp + ys, 0),
                        ((off >= 0) & (z >= 1), me_sp - ys, 1),
                        (y + 1 < ys, me_sp + 1, 2),
                        (y >= 1, me_sp - 1, 3),
                    ),
                    drain,
                )

    def ypart(k, ws, drain=False, then=None):
        sz = z + offset(k)

        @pl.when((sz >= 0) & (sz < zs))
        def _():
            for j in range(1, 2 * ys - 1):
                yoff = ((j + 1) // 2) * (1 - 2 * (j % 2))
                sy = y + yoff

                @pl.when((sy >= 0) & (sy < ys))
                def _():
                    s = sz * ys + sy
                    for w in ws:
                        if not drain:
                            piece(w, s, me_sp, 0).wait_recv()
                        if yoff < 0:
                            moves = ((y + 1 < ys, me_sp + 1, 2),)
                        else:
                            moves = ((y >= 1, me_sp - 1, 3),)
                        send_all(w, s, moves, drain)
                    if then is not None:
                        then(s)

    def loop(lo, hi, body):
        def step(k, carry):
            body(k)
            return carry

        lax.fori_loop(lo, hi, step, 0)

    locals_in = [
        pltpu.make_async_copy(
            source, weights.at[w, block_rows(me_sp, chunk), :], local_sem.at[w]
        )
        for w, source in enumerate((gate_hbm, up_hbm, down_hbm))
    ]
    res_in = pltpu.make_async_copy(res_hbm.at[own_rows, :], res, local_sem.at[3])
    for copy in locals_in:
        copy.start()
    res_in.start()

    def halo(i, source, target):
        return pltpu.make_async_remote_copy(
            src_ref=source.at[pl.ds(rows - WINDOW, WINDOW), :],
            dst_ref=target.at[pl.ds(0, WINDOW), :],
            send_sem=halo_send.at[i],
            recv_sem=halo_recv.at[i],
            device_id={"sp": me_sp + 1},
            device_id_type=MESH,
        )

    halos = ((0, k_ref, kext), (1, v_ref, vext))

    @pl.when(me_sp + 1 < sp)
    def _():
        for h in halos:
            halo(*h).start()

    locals_in[GATE].wait()
    locals_in[UP].wait()
    zpart(0, (GATE, UP))

    @pl.when(me_sp == 0)
    def _():
        kext[pl.ds(0, WINDOW), :] = jnp.zeros((WINDOW, kext.shape[1]), kext.dtype)
        vext[pl.ds(0, WINDOW), :] = jnp.zeros((WINDOW, vext.shape[1]), vext.dtype)

    kext[pl.ds(WINDOW, rows), :] = k_ref[...]
    vext[pl.ds(WINDOW, rows), :] = v_ref[...]
    qi = lax.broadcasted_iota(jnp.int32, (WINDOW, 2 * WINDOW), 0)
    ki = lax.broadcasted_iota(jnp.int32, (WINDOW, 2 * WINDOW), 1)
    distance = qi - ki + WINDOW
    distance_f = distance.astype(jnp.float32)
    in_window = (distance >= 0) & (distance < WINDOW)
    base_head = (me * heads).astype(jnp.float32)

    def attend(n):
        q_rows = block_rows(n, WINDOW)
        band = pl.ds(pl.multiple_of(n * WINDOW, WINDOW), 2 * WINDOW)
        place = me_sp * rows + n * WINDOW - WINDOW + ki
        valid = in_window & (place >= 0)
        outs = []
        for h in range(heads):
            kv = h // groups
            qh = q_ref[q_rows, h * HD : (h + 1) * HD]
            kh = kext[band, kv * HD : (kv + 1) * HD]
            vh = vext[band, kv * HD : (kv + 1) * HD]
            score = lax.dot_general(
                qh, kh, (((1,), (1,)), ((), ())), preferred_element_type=jnp.float32
            )
            exponent = jnp.full((1, 2 * WINDOW), base_head + (h + 1), jnp.float32)
            slope = jnp.exp2(exponent * (-8.0 / QH))
            score = score * HD ** (-0.5) - slope * distance_f
            score = jnp.where(valid, score, -jnp.inf)
            sink = sink_ref[h]
            top = jnp.maximum(jnp.max(score, axis=-1, keepdims=True), sink)
            expd = jnp.exp(score - top)
            denom = jnp.sum(expd, axis=-1, keepdims=True) + jnp.exp(sink - top)
            prob = (expd / denom).astype(jnp.bfloat16)
            outs.append(jnp.dot(prob, vh, preferred_element_type=jnp.float32))
        att[q_rows, :] = jnp.concatenate(outs, axis=1).astype(jnp.bfloat16)

    loop(1, blocks, attend)

    @pl.when(me_sp > 0)
    def _():
        for h in halos:
            halo(*h).wait_recv()

    attend(0)

    def to_owner(u):
        return pltpu.make_async_remote_copy(
            src_ref=psend.at[block_rows(u, own), :],
            dst_ref=precv.at[me],
            send_sem=rs_send.at[u],
            recv_sem=rs_recv.at[me],
            device_id={"tp": u},
            device_id_type=MESH,
        )

    def from_peer(t):
        return pltpu.make_async_remote_copy(
            src_ref=psend.at[own_rows, :],
            dst_ref=precv.at[t],
            send_sem=rs_send.at[t],
            recv_sem=rs_recv.at[t],
            device_id={"tp": t},
            device_id_type=MESH,
        )

    def project(j):
        u = (me + 1 + j) % tp
        u_rows = block_rows(u, own)
        psend[u_rows, :] = jnp.dot(
            att[u_rows, :], ow_ref[...], preferred_element_type=jnp.float32
        ).astype(jnp.bfloat16)

        @pl.when(j < tp - 1)
        def _():
            to_owner(u).start()

    loop(0, tp, project)

    def relay_gu(k):
        zpart(k, (GATE, UP))

        @pl.when(k >= LAG)
        def _():
            ypart(k - LAG, (GATE, UP))

    middle = min(5, last + 1)
    loop(1, middle, relay_gu)

    res_in.wait()
    for j in range(tp - 1):
        from_peer((me + 1 + j) % tp).wait_recv()
    tile = 32

    def norm_tile(i):
        t_rows = block_rows(i, tile)
        total = psend[pl.ds(pl.multiple_of(me * own + i * tile, tile), tile), :].astype(
            jnp.float32
        )
        for j in range(tp - 1):
            total = total + precv[(me + 1 + j) % tp, t_rows, :].astype(jnp.float32)
        mix = (res[t_rows, :].astype(jnp.float32) + total).astype(jnp.bfloat16)
        mixed[t_rows, :] = mix
        mix_f = mix.astype(jnp.float32)
        scale = lax.rsqrt(jnp.mean(mix_f * mix_f, axis=-1, keepdims=True) + 1e-06)
        normed[pl.ds(pl.multiple_of(me * own + i * tile, tile), tile), :] = (
            mix_f * scale * gain_ref[...]
        ).astype(jnp.bfloat16)

    loop(0, own // tile, norm_tile)

    def hand(block, peer):
        part = normed.at[block_rows(block, own), :]
        return pltpu.make_async_remote_copy(
            src_ref=part,
            dst_ref=part,
            send_sem=ag_send.at[peer],
            recv_sem=ag_recv.at[block],
            device_id={"tp": peer},
            device_id_type=MESH,
        )

    for j in range(tp - 1):
        hand(me, (me + 1 + j) % tp).start()

    loop(middle, last + 1, relay_gu)
    locals_in[DOWN].wait()
    zpart(0, (DOWN,))
    loop(last + 1 - LAG, last + 1, lambda k: ypart(k, (GATE, UP)))
    loop(1, 3, lambda k: zpart(k, (DOWN,)))

    def expand(j):
        u = (me + j) % tp

        @pl.when(j > 0)
        def _():
            hand(u, u).wait_recv()

        u_rows = block_rows(u, own)
        part = normed[u_rows, :]
        gate = jnp.dot(part, weights[GATE], preferred_element_type=jnp.float32)
        upper = jnp.dot(part, weights[UP], preferred_element_type=jnp.float32)
        hidden[u_rows, :] = (gate / (1.0 + jnp.exp(-gate)) * upper).astype(jnp.bfloat16)

    loop(0, tp, expand)

    def ex_copy(sender, u, s):
        return pltpu.make_async_remote_copy(
            src_ref=esend.at[s, block_rows(u, own), :],
            dst_ref=erecv.at[sender, s],
            send_sem=ex_send.at[u, s],
            recv_sem=ex_recv.at[sender, s],
            device_id={"tp": u},
            device_id_type=MESH,
        )

    def contract(s):
        block = weights[DOWN, block_rows(s, chunk), :]

        def one(j):
            u = (me + 1 + j) % tp
            u_rows = block_rows(u, own)
            esend[s, u_rows, :] = lax.dot_general(
                hidden[u_rows, :],
                block,
                (((1,), (1,)), ((), ())),
                preferred_element_type=jnp.float32,
            ).astype(jnp.bfloat16)

            @pl.when(j < tp - 1)
            def _():
                ex_copy(me, u, s).start()

        loop(0, tp, one)

    def relay_down(k):
        @pl.when((k >= 3) & (k <= last))
        def _():
            zpart(k, (DOWN,))

        sz = z + offset(k)

        @pl.when((k <= last) & (sz >= 0) & (sz < zs))
        def _():
            contract(sz * ys + y)

        @pl.when(k >= LAG)
        def _():
            ypart(k - LAG, (DOWN,), then=contract)

    loop(0, last + 1 + LAG, relay_down)

    for s in range(sp):
        cols = slice(s * chunk, (s + 1) * chunk)
        total = esend[s, own_rows, :].astype(jnp.float32)
        for j in range(tp - 1):
            t = (me + 1 + j) % tp
            ex_copy(t, t, s).wait_recv()
            total = total + erecv[t, s].astype(jnp.float32)
        out_ref[:, cols] = (mixed[:, cols].astype(jnp.float32) + 0.5 * total).astype(
            jnp.bfloat16
        )

    @pl.when(me_sp + 1 < sp)
    def _():
        for h in halos:
            halo(*h).wait_send()

    def drain(k):
        zpart(k, (GATE, UP, DOWN), drain=True)
        ypart(k, (GATE, UP, DOWN), drain=True)

    loop(0, last + 1, drain)

    def drain_peer(j):
        u = (me + 1 + j) % tp
        to_owner(u).wait_send()
        hand(me, u).wait_send()
        loop(0, sp, lambda s: ex_copy(me, u, s).wait_send())

    loop(0, tp - 1, drain_peer)


def per_device(
    zs,
    ys,
    tp,
    queries,
    keys,
    values,
    sink_logits,
    residual,
    out_weight,
    norm_gain,
    gate_weight,
    up_weight,
    down_weight,
):
    sp = zs * ys
    rows, width = residual.shape
    own = rows // tp
    chunk, units = gate_weight.shape
    vmem = pl.BlockSpec(memory_space=pltpu.VMEM)
    hbm = pl.BlockSpec(memory_space=pl.ANY)
    dma = pltpu.SemaphoreType.DMA
    bf16 = jnp.bfloat16
    return pl.pallas_call(
        functools.partial(layer_kernel, zs, ys, tp),
        out_shape=jax.ShapeDtypeStruct((own, width), bf16),
        in_specs=[
            vmem,
            vmem,
            vmem,
            pl.BlockSpec(memory_space=pltpu.SMEM),
            hbm,
            vmem,
            vmem,
            hbm,
            hbm,
            hbm,
        ],
        out_specs=vmem,
        scratch_shapes=[
            pltpu.VMEM((3, sp * chunk, units), bf16),
            pltpu.VMEM((rows + WINDOW, keys.shape[1]), bf16),
            pltpu.VMEM((rows + WINDOW, values.shape[1]), bf16),
            pltpu.VMEM((rows, queries.shape[1]), bf16),
            pltpu.VMEM((rows, width), bf16),
            pltpu.VMEM((tp, own, width), bf16),
            pltpu.VMEM((own, width), bf16),
            pltpu.VMEM((own, width), bf16),
            pltpu.VMEM((rows, width), bf16),
            pltpu.VMEM((rows, units), bf16),
            pltpu.VMEM((sp, rows, chunk), bf16),
            pltpu.VMEM((tp, sp, own, chunk), bf16),
            dma((4,)),
            dma((2,)),
            dma((2,)),
            dma((3, sp, 4)),
            dma((3, sp)),
            dma((tp,)),
            dma((tp,)),
            dma((tp,)),
            dma((tp,)),
            dma((tp, sp)),
            dma((tp, sp)),
        ],
        compiler_params=pltpu.CompilerParams(
            has_side_effects=True, vmem_limit_bytes=67_000_000
        ),
    )(
        queries,
        keys,
        values,
        sink_logits,
        residual,
        out_weight,
        norm_gain.reshape(1, width),
        gate_weight,
        up_weight,
        down_weight,
    )


def solution(mesh):
    tp = mesh.shape["tp"]
    sp = mesh.shape["sp"]
    ys = max(tp // 2, 1)
    if sp % ys:
        ys = 1
    return jax.shard_map(
        functools.partial(per_device, sp // ys, ys, tp),
        mesh=mesh,
        in_specs=(
            P("sp", "tp"),
            P("sp", "tp"),
            P("sp", "tp"),
            P("tp"),
            P("sp", None),
            P("tp", None),
            P(),
            P("sp", "tp"),
            P("sp", "tp"),
            P("sp", "tp"),
        ),
        out_specs=P(("sp", "tp"), None),
        check_vma=False,
    )
```

time: 387 us -> 220 us (0.57)
  waiting for transfers between devices: 303 us -> 0 us
  Pallas kernels: 0 us -> 218 us
  matrix products: 41.9 us -> 0 us
  between operations: 15.2 us -> 0.01 us
  other arithmetic: 12.5 us -> 0 us
  local copies, waits for them, and re-layouts: 8.71 us -> 2.3 us
  starting transfers between devices: 4.31 us -> 0 us
    pallas_call x0 -> x1, Pallas kernels: none -> 218 us  [per_device(): pl.pallas_call(functools.partial(layer_kernel, zs, ys, tp), out_shape=jax...]
    all_gather x3 -> x0, waiting for transfers between devices: 173 us -> none  [the longest x1 92.4 us: per_device(): down_full = lax.all_gather(down_weight, 'sp', axis=0, tiled=True)]
    psum x1 -> x0, waiting for transfers between devices: 83.9 us -> none  [per_device(): lax.psum(partial_sum.astype(jnp.bfloat16), 'tp').astype(jnp.float32)]
    reduce_scatter x1 -> x0, waiting for transfers between devices: 44.4 us -> none  [per_device(): lax.psum_scatter(lax.dot_general(hidden, down_full, (((1,), (1,)), ((), (...]
    dot_general x5 -> x0, matrix products: 41.9 us -> none  [the longest x1 20.8 us: per_device(): lax.dot_general(hidden, down_full, (((1,), (1,)), ((), ())), preferred_el...]
    reduce_sum x2 -> x0, other arithmetic: 8.57 us -> none  [the longest x1 7.46 us: rms_scale(): scale = lax.rsqrt(jnp.mean(rows_f * rows_f, axis=-1, keepdims=True) + 1e-06)]
    ppermute x1 -> x0, starting transfers between devices: 3.96 us -> none  [shifted(): return lax.ppermute(block, axis, route)]
  transfers between devices with their start and end apart: 6 -> 0, of which waited for: 5 -> 0; matrix products, arithmetic and copies ran while one was open for 6% -> 0% of each run, Pallas kernels for 0% -> 0%
where the time goes in v1:
time: 220 us
  Pallas kernels  218 us (99%)
  local copies, waits for them, and re-layouts  2.3 us (1%)
    pallas_call x1, Pallas kernels, per_device(): pl.pallas_call(functools.partial(layer_kernel, zs, ys, tp), out_shape=jax...  218 us

profile of v1, /device:TPU:1, one launch (start us, length us, event | category | flops | bytes accessed | tf_op | source)
XLA Modules:
  0.0 220.2 jit_solution(10009761732702424002)
XLA Ops:
  0.0 217.9 %shard_map.100 = bf16[256,2048]{1,0:T(8,128)(2,1)} custom-call(bf16[1024,256]{1,0:T(8,128)(2,1)} %q_ref.1, bf16[1024,128]{1,0:T(8,128)(2,1)} %k_ref.1, bf16[1024,128]{1,0:T(8,128)(2,1)} %v_ref.1, f32[4]{0:T(128)} %sink_ref.1, bf16[1024,2048]{1,0:T(8,128)(2,1)} %res_hbm.1, bf16[256,2048]{1,0:T(8,128)(2,1)} %ow_ref.1, f32[1,2048]{1,0:T(1,128)} %bitcast.1, ...), custom_call_target="tpu_custom_call" | custom-call | tf_op jit(solution)/shard_map/pallas_call | solution.py:438
  217.9 2.3 %copy.12 = bf16[256,2048]{1,0:T(8,128)(2,1)} copy(bf16[256,2048]{1,0:T(8,128)(2,1)} %shard_map.100) | data formatting | bytes 2097152

commit v2 on v1

--- a/solution.py
+++ b/solution.py
@@ -11,7 +11,7 @@
 HD = 64
 WINDOW = 128
 LAG = 2
-GATE, UP, DOWN = 0, 1, 2
+GATE, UP, DOWN_A, DOWN_B = 0, 1, 2, 3
 MESH = pl.DeviceIdType.MESH
 
 
@@ -19,6 +19,7 @@
     zs,
     ys,
     tp,
+    halves,
     q_ref,
     k_ref,
     v_ref,
@@ -31,6 +32,7 @@
     down_hbm,
     out_ref,
     weights,
+    downs,
     kext,
     vext,
     att,
@@ -63,6 +65,8 @@
     rows = q_ref.shape[0]
     own = rows // tp
     chunk = gate_hbm.shape[0]
+    half = chunk // halves
+    split = halves == 2
     heads = q_ref.shape[1] // HD
     kvs = k_ref.shape[1] // HD
     groups = heads // kvs
@@ -73,8 +77,13 @@
 
     own_rows = block_rows(me, own)
 
+    def part_of(w, s):
+        if w >= DOWN_A:
+            return downs.at[w - DOWN_A, block_rows(s, half), :]
+        return weights.at[w, block_rows(s, chunk), :]
+
     def piece(w, s, target, direction):
-        part = weights.at[w, block_rows(s, chunk), :]
+        part = part_of(w, s)
         return pltpu.make_async_remote_copy(
             src_ref=part,
             dst_ref=part,
@@ -147,6 +156,55 @@
                     if then is not None:
                         then(s)
 
+    def along_z(k, s, w, drain):
+        off = offset(k)
+        send_all(
+            w,
+            s,
+            (
+                ((off <= 0) & (z + 1 < zs), me_sp + ys, 0),
+                ((off >= 0) & (z >= 1), me_sp - ys, 1),
+            ),
+            drain,
+        )
+
+    def yfirst(first, end, drain=False):
+        for j in range(first, end):
+            yoff = ((j + 1) // 2) * (1 - 2 * (j % 2))
+            sy = y + yoff
+
+            @pl.when((sy >= 0) & (sy < ys))
+            def _():
+                s = z * ys + sy
+                if not drain and j > 0:
+                    piece(DOWN_B, s, me_sp, 0).wait_recv()
+                moves = ()
+                if yoff <= 0:
+                    moves += ((y + 1 < ys, me_sp + 1, 2),)
+                if yoff >= 0:
+                    moves += ((y >= 1, me_sp - 1, 3),)
+                send_all(DOWN_B, s, moves, drain)
+
+    def zsecond(k, drain=False):
+        sz = z + offset(k)
+
+        @pl.when((sz >= 0) & (sz < zs))
+        def _():
+            for sy in range(ys):
+                s = sz * ys + sy
+                if not drain:
+
+                    @pl.when(k > 0)
+                    def _():
+                        piece(DOWN_B, s, me_sp, 0).wait_recv()
+
+                along_z(k, s, DOWN_B, drain)
+
+    def zdown(k):
+        zpart(k, (DOWN_A,))
+        if split:
+            zsecond(k)
+
     def loop(lo, hi, body):
         def step(k, carry):
             body(k)
@@ -156,11 +214,18 @@
 
     locals_in = [
         pltpu.make_async_copy(
-            source, weights.at[w, block_rows(me_sp, chunk), :], local_sem.at[w]
-        )
-        for w, source in enumerate((gate_hbm, up_hbm, down_hbm))
+            source, part_of(w, me_sp), local_sem.at[w]
+        )
+        for w, source in enumerate((gate_hbm, up_hbm))
+    ] + [
+        pltpu.make_async_copy(
+            down_hbm.at[pl.ds(h * half, half), :],
+            part_of(DOWN_A + h, me_sp),
+            local_sem.at[DOWN_A + h],
+        )
+        for h in range(halves)
     ]
-    res_in = pltpu.make_async_copy(res_hbm.at[own_rows, :], res, local_sem.at[3])
+    res_in = pltpu.make_async_copy(res_hbm.at[own_rows, :], res, local_sem.at[4])
     for copy in locals_in:
         copy.start()
     res_in.start()
@@ -185,6 +250,10 @@
     locals_in[GATE].wait()
     locals_in[UP].wait()
     zpart(0, (GATE, UP))
+    for h in range(halves):
+        locals_in[DOWN_A + h].wait()
+    if split:
+        yfirst(0, 1)
 
     @pl.when(me_sp == 0)
     def _():
@@ -278,6 +347,9 @@
     middle = min(5, last + 1)
     loop(1, middle, relay_gu)
 
+    if split:
+        yfirst(1, 2 * ys - 1)
+
     res_in.wait()
     for j in range(tp - 1):
         from_peer((me + 1 + j) % tp).wait_recv()
@@ -315,10 +387,8 @@
         hand(me, (me + 1 + j) % tp).start()
 
     loop(middle, last + 1, relay_gu)
-    locals_in[DOWN].wait()
-    zpart(0, (DOWN,))
+    loop(0, 3, zdown)
     loop(last + 1 - LAG, last + 1, lambda k: ypart(k, (GATE, UP)))
-    loop(1, 3, lambda k: zpart(k, (DOWN,)))
 
     def expand(j):
         u = (me + j) % tp
@@ -326,6 +396,10 @@
         @pl.when(j > 0)
         def _():
             hand(u, u).wait_recv()
+
+        @pl.when(j == tp // 2)
+        def _():
+            loop(3, 5, zdown)
 
         u_rows = block_rows(u, own)
         part = normed[u_rows, :]
@@ -345,13 +419,14 @@
             device_id_type=MESH,
         )
 
-    def contract(s):
-        block = weights[DOWN, block_rows(s, chunk), :]
+    def contract(h, sz):
+        part = h * zs + sz
+        block = downs[h, block_rows(sz, ys * half), :]
 
         def one(j):
             u = (me + 1 + j) % tp
             u_rows = block_rows(u, own)
-            esend[s, u_rows, :] = lax.dot_general(
+            esend[part, u_rows, :] = lax.dot_general(
                 hidden[u_rows, :],
                 block,
                 (((1,), (1,)), ((), ())),
@@ -360,37 +435,47 @@
 
             @pl.when(j < tp - 1)
             def _():
-                ex_copy(me, u, s).start()
+                ex_copy(me, u, part).start()
 
         loop(0, tp, one)
 
     def relay_down(k):
-        @pl.when((k >= 3) & (k <= last))
-        def _():
-            zpart(k, (DOWN,))
-
-        sz = z + offset(k)
-
-        @pl.when((k <= last) & (sz >= 0) & (sz < zs))
-        def _():
-            contract(sz * ys + y)
+        @pl.when((k >= 5) & (k <= last))
+        def _():
+            zdown(k)
+
+        if split:
+            sz = z + offset(k)
+
+            @pl.when((k <= last) & (sz >= 0) & (sz < zs))
+            def _():
+                contract(1, sz)
 
         @pl.when(k >= LAG)
         def _():
-            ypart(k - LAG, (DOWN,), then=contract)
+            ypart(k - LAG, (DOWN_A,))
+            sy = z + offset(k - LAG)
+
+            @pl.when((sy >= 0) & (sy < zs))
+            def _():
+                contract(0, sy)
 
     loop(0, last + 1 + LAG, relay_down)
 
-    for s in range(sp):
-        cols = slice(s * chunk, (s + 1) * chunk)
-        total = esend[s, own_rows, :].astype(jnp.float32)
+    for part in range(halves * zs):
+        h, sz = divmod(part, zs)
+        total = esend[part, own_rows, :].astype(jnp.float32)
         for j in range(tp - 1):
             t = (me + 1 + j) % tp
-            ex_copy(t, t, s).wait_recv()
-            total = total + erecv[t, s].astype(jnp.float32)
-        out_ref[:, cols] = (mixed[:, cols].astype(jnp.float32) + 0.5 * total).astype(
-            jnp.bfloat16
-        )
+            ex_copy(t, t, part).wait_recv()
+            total = total + erecv[t, part].astype(jnp.float32)
+        for sy in range(ys):
+            first = (sz * ys + sy) * chunk + h * half
+            cols = slice(first, first + half)
+            out_ref[:, cols] = (
+                mixed[:, cols].astype(jnp.float32)
+                + 0.5 * total[:, sy * half : (sy + 1) * half]
+            ).astype(jnp.bfloat16)
 
     @pl.when(me_sp + 1 < sp)
     def _():
@@ -398,16 +483,20 @@
             halo(*h).wait_send()
 
     def drain(k):
-        zpart(k, (GATE, UP, DOWN), drain=True)
-        ypart(k, (GATE, UP, DOWN), drain=True)
+        zpart(k, (GATE, UP, DOWN_A), drain=True)
+        ypart(k, (GATE, UP, DOWN_A), drain=True)
+        if split:
+            zsecond(k, drain=True)
 
     loop(0, last + 1, drain)
+    if split:
+        yfirst(0, 2 * ys - 1, drain=True)
 
     def drain_peer(j):
         u = (me + 1 + j) % tp
         to_owner(u).wait_send()
         hand(me, u).wait_send()
-        loop(0, sp, lambda s: ex_copy(me, u, s).wait_send())
+        loop(0, halves * zs, lambda s: ex_copy(me, u, s).wait_send())
 
     loop(0, tp - 1, drain_peer)
 
@@ -431,12 +520,14 @@
     rows, width = residual.shape
     own = rows // tp
     chunk, units = gate_weight.shape
+    halves = 2 if chunk % 256 == 0 else 1
+    half = chunk // halves
     vmem = pl.BlockSpec(memory_space=pltpu.VMEM)
     hbm = pl.BlockSpec(memory_space=pl.ANY)
     dma = pltpu.SemaphoreType.DMA
     bf16 = jnp.bfloat16
     return pl.pallas_call(
-        functools.partial(layer_kernel, zs, ys, tp),
+        functools.partial(layer_kernel, zs, ys, tp, halves),
         out_shape=jax.ShapeDtypeStruct((own, width), bf16),
         in_specs=[
             vmem,
@@ -452,7 +543,8 @@
         ],
         out_specs=vmem,
         scratch_shapes=[
-            pltpu.VMEM((3, sp * chunk, units), bf16),
+            pltpu.VMEM((2, sp * chunk, units), bf16),
+            pltpu.VMEM((halves, sp * half, units), bf16),
             pltpu.VMEM((rows + WINDOW, keys.shape[1]), bf16),
             pltpu.VMEM((rows + WINDOW, values.shape[1]), bf16),
             pltpu.VMEM((rows, queries.shape[1]), bf16),
@@ -462,19 +554,19 @@
             pltpu.VMEM((own, width), bf16),
             pltpu.VMEM((rows, width), bf16),
             pltpu.VMEM((rows, units), bf16),
-            pltpu.VMEM((sp, rows, chunk), bf16),
-            pltpu.VMEM((tp, sp, own, chunk), bf16),
-            dma((4,)),
+            pltpu.VMEM((halves * zs, rows, ys * half), bf16),
+            pltpu.VMEM((tp, halves * zs, own, ys * half), bf16),
+            dma((5,)),
             dma((2,)),
             dma((2,)),
-            dma((3, sp, 4)),
-            dma((3, sp)),
+            dma((2 + halves, sp, 4)),
+            dma((2 + halves, sp)),
             dma((tp,)),
             dma((tp,)),
             dma((tp,)),
             dma((tp,)),
-            dma((tp, sp)),
-            dma((tp, sp)),
+            dma((tp, halves * zs)),
+            dma((tp, halves * zs)),
         ],
         compiler_params=pltpu.CompilerParams(
             has_side_effects=True, vmem_limit_bytes=67_000_000

time: 220 us -> 252 us (1.15)
  Pallas kernels: 218 us -> 250 us
    pallas_call x1, Pallas kernels: 218 us -> 250 us  [per_device(): pl.pallas_call(functools.partial(layer_kernel, zs, ys, tp, halves), out_s...]
where the time goes in v2:
time: 252 us
  Pallas kernels  250 us (99%)
    pallas_call x1, Pallas kernels, per_device(): pl.pallas_call(functools.partial(layer_kernel, zs, ys, tp, halves), out_s...  250 us

profile of v2, /device:TPU:1, one launch (start us, length us, event | category | flops | bytes accessed | tf_op | source)
XLA Modules:
  0.0 252.2 jit_solution(15925886474306196767)
XLA Ops:
  0.0 249.9 %shard_map.100 = bf16[256,2048]{1,0:T(8,128)(2,1)} custom-call(bf16[1024,256]{1,0:T(8,128)(2,1)} %q_ref.1, bf16[1024,128]{1,0:T(8,128)(2,1)} %k_ref.1, bf16[1024,128]{1,0:T(8,128)(2,1)} %v_ref.1, f32[4]{0:T(128)} %sink_ref.1, bf16[1024,2048]{1,0:T(8,128)(2,1)} %res_hbm.1, bf16[256,2048]{1,0:T(8,128)(2,1)} %ow_ref.1, f32[1,2048]{1,0:T(1,128)} %bitcast.1, ...), custom_call_target="tpu_custom_call" | custom-call | tf_op jit(solution)/shard_map/pallas_call | solution.py:529
  249.9 2.3 copy.12

commit v3 on v2

--- a/solution.py
+++ b/solution.py
@@ -340,10 +340,6 @@
     def relay_gu(k):
         zpart(k, (GATE, UP))
 
-        @pl.when(k >= LAG)
-        def _():
-            ypart(k - LAG, (GATE, UP))
-
     middle = min(5, last + 1)
     loop(1, middle, relay_gu)
 
@@ -388,7 +384,7 @@
 
     loop(middle, last + 1, relay_gu)
     loop(0, 3, zdown)
-    loop(last + 1 - LAG, last + 1, lambda k: ypart(k, (GATE, UP)))
+    loop(0, last + 1, lambda k: ypart(k, (GATE, UP)))
 
     def expand(j):
         u = (me + j) % tp

time: 252 us -> 211 us (0.84)
  Pallas kernels: 250 us -> 209 us
    pallas_call x1, Pallas kernels: 250 us -> 209 us  [per_device(): pl.pallas_call(functools.partial(layer_kernel, zs, ys, tp, halves), out_s...]
where the time goes in v3:
time: 211 us
  Pallas kernels  209 us (99%)
  local copies, waits for them, and re-layouts  2.3 us (1%)
    pallas_call x1, Pallas kernels, per_device(): pl.pallas_call(functools.partial(layer_kernel, zs, ys, tp, halves), out_s...  209 us

profile of v3, /device:TPU:1, one launch (start us, length us, event | category | flops | bytes accessed | tf_op | source)
XLA Modules:
  0.0 211.2 jit_solution(5723741057447711091)
XLA Ops:
  0.0 208.9 %shard_map.100 = bf16[256,2048]{1,0:T(8,128)(2,1)} custom-call(bf16[1024,256]{1,0:T(8,128)(2,1)} %q_ref.1, bf16[1024,128]{1,0:T(8,128)(2,1)} %k_ref.1, bf16[1024,128]{1,0:T(8,128)(2,1)} %v_ref.1, f32[4]{0:T(128)} %sink_ref.1, bf16[1024,2048]{1,0:T(8,128)(2,1)} %res_hbm.1, bf16[256,2048]{1,0:T(8,128)(2,1)} %ow_ref.1, f32[1,2048]{1,0:T(1,128)} %bitcast.1, ...), custom_call_target="tpu_custom_call" | custom-call | tf_op jit(solution)/shard_map/pallas_call | solution.py:525
  208.9 2.3 %copy.12 = bf16[256,2048]{1,0:T(8,128)(2,1)} copy(bf16[256,2048]{1,0:T(8,128)(2,1)} %shard_map.100) | data formatting | bytes 2097152
